TPU v7x, 32 devices: a whole 2x2x4 slice. The times are simulated.
32 devices in a mesh: ep: 8 (over z, x), tp: 4 (over y, core).
Axes of the slice: x: 2, y: 2, z: 4, core: 2. Of those that a mesh axis runs over, the one named last changes fastest.
Arguments:
- residual: bfloat16 [64, 2048], P(None, 'ep'), may hold values from -40 to 40
- norm_gain: float32 [2048], P('ep'), may hold values from 0.1 to 1.9
- query_weight: bfloat16 [2048, 2048], P('ep', 'tp'), may hold values from -0.125 to 0.125
- key_weight: bfloat16 [2048, 2048], P('ep', 'tp'), may hold values from -0.125 to 0.125
- value_weight: bfloat16 [2048, 4096], P('ep', 'tp'), may hold values from -0.125 to 0.125
- gate_weight: bfloat16 [2048, 4096], P('ep', 'tp'), may hold values from -0.125 to 0.125
- out_weight: bfloat16 [4096, 2048], P('tp', 'ep'), may hold values from -0.09375 to 0.09375
- prior_state: float32 [64, 16, 128, 256], P('ep', 'tp'), may hold values from -3 to 3
- lengths: int32 [64], P('ep'), may hold values from 1024 to 16383
- ffn_gain: float32 [2048], replicated, may hold values from 0.1 to 1.9
- expert_gate: bfloat16 [8, 2048, 2048], P('ep', None, 'tp'), may hold values from -0.5 to 0.5
- expert_up: bfloat16 [8, 2048, 2048], P('ep', None, 'tp'), may hold values from -0.5 to 0.5
- expert_down: bfloat16 [8, 2048, 2048], P('ep', 'tp'), may hold values from -0.03125 to 0.03125
- route_ids: int32 [64, 4], replicated, may hold values from 0 to 7, all different within a row; in each aligned block of 8 rows (0 to 7, 8 to 15, ...) at most 8 rows name the same one
- route_weight: float32 [64, 4], replicated, may hold values from 0.1 to 1
- dense_gate: bfloat16 [2048, 2048], P('ep', 'tp'), may hold values from -0.125 to 0.125
- dense_up: bfloat16 [2048, 2048], P('ep', 'tp'), may hold values from -0.125 to 0.125
- dense_down: bfloat16 [2048, 2048], P('tp', 'ep'), may hold values from -0.1875 to 0.1875
- mix_vector: bfloat16 [2048], P('ep'), may hold values from -0.125 to 0.125
Outputs:
- layer_out: bfloat16 [64, 2048], P(None, 'ep')
- new_state: float32 [64, 16, 128, 256], P('ep', 'tp')
Inputs may be any that keep to these rules, and one draw needn't show every extreme that they name: `route_ids`: each row names 4 different experts; within each aligned block of 8 rows no expert is named by more than 8 rows, and in some block one expert is named by exactly 8 rows.
All inputs are finite; a program needn't handle non-finite values.
Results may differ from a plain program's by a relative error of at most 0.02.
Values may be sent and summed in bfloat16 or wider, within the bound.
A program may use at most 64 MiB of HBM per device.

v0:
```python
import jax
import jax.numpy as jnp
from jax import lax
from jax.sharding import PartitionSpec as P

D = 2048
KEY_DIM = 128
VAL_DIM = 256


norm_eps = 1e-06
clamp_limit = 7.0
gate_alpha = 1.702


def rotate_half(vectors, positions):
    half_dim = vectors.shape[-1] // 2
    inverse = 1.0 / 10000.0 ** jnp.linspace(0.0, 1.0, half_dim, dtype=jnp.float32)
    angles = positions.astype(jnp.float32)[:, None] * inverse[None, :]
    cosine = jnp.cos(angles)[:, None, :]
    sine_part = jnp.sin(angles)[:, None, :]
    first_half = vectors[..., :half_dim]
    second_half = vectors[..., half_dim:]
    return jnp.concatenate(
        [
            first_half * cosine - second_half * sine_part,
            second_half * cosine + first_half * sine_part,
        ],
        axis=-1,
    )


def slot_index(route_ids, groups, capacity, experts):
    pair_ids = route_ids.reshape(groups, -1)
    labels = jnp.arange(experts, dtype=jnp.int32)
    onehot = (pair_ids[:, :, None] == labels[None, None, :]).astype(jnp.int32)
    earlier = jnp.cumsum(onehot, axis=1) - onehot
    within = jnp.sum(earlier * onehot, axis=2)
    offset = jnp.arange(groups, dtype=jnp.int32)[:, None] * capacity
    return (pair_ids * (groups * capacity) + offset + within).reshape(-1)


def source_rows(target, total_rows, topk_count, table_size):
    owners = jnp.arange(target.shape[0], dtype=jnp.int32) // topk_count
    return jnp.full((table_size,), total_rows, jnp.int32).at[target].set(owners)


def rounded_product(left_rows, right_rows):
    partial_value = jnp.dot(left_rows, right_rows, preferred_element_type=jnp.float32)
    return lax.optimization_barrier(partial_value.astype(jnp.bfloat16))


def per_device(
    residual,
    norm_gain,
    query_weight,
    key_weight,
    value_weight,
    gate_weight,
    out_weight,
    prior_state,
    lengths,
    ffn_gain,
    expert_gate,
    expert_up,
    expert_down,
    route_ids,
    route_weight,
    dense_gate,
    dense_up,
    dense_down,
    mix_vector,
):
    ep_count = lax.axis_size("ep")
    ep_index = lax.axis_index("ep")
    batch_rows, local_width = residual.shape
    own_rows = batch_rows // ep_count
    topk_count = route_ids.shape[1]
    residual_float = residual.astype(jnp.float32)
    squares = jnp.sum(residual_float * residual_float, axis=1)
    normed_in = (residual_float * norm_gain).astype(jnp.bfloat16)
    all_weights = jnp.concatenate([query_weight, key_weight, value_weight, gate_weight], axis=1)
    whole_terms = jnp.dot(normed_in, all_weights, preferred_element_type=jnp.float32)
    projected, own_squares = (
        lax.psum_scatter(whole_terms, "ep", scatter_dimension=0, tiled=True),
        lax.psum_scatter(squares, "ep", scatter_dimension=0, tiled=True),
    )
    row_scale = lax.rsqrt(own_squares / D + norm_eps)[:, None]
    key_cols = query_weight.shape[1]
    value_cols = value_weight.shape[1]
    heads_here = key_cols // KEY_DIM
    projected = projected * row_scale
    query_rot = rotate_half(projected[:, :key_cols].reshape(own_rows, heads_here, KEY_DIM), lengths)
    key_rot = rotate_half(
        projected[:, key_cols : 2 * key_cols].reshape(own_rows, heads_here, KEY_DIM), lengths
    ) * KEY_DIM ** (-0.5)
    values = projected[:, 2 * key_cols : 2 * key_cols + value_cols].reshape(
        own_rows, heads_here, VAL_DIM
    )
    gate_pre = projected[:, 2 * key_cols + value_cols :].reshape(own_rows, heads_here, VAL_DIM)
    head_ids = lax.axis_index("tp") * heads_here + jnp.arange(heads_here, dtype=jnp.int32)
    decay_rate = 1.0 - jnp.exp2(-1.0 - 0.5 * head_ids.astype(jnp.float32))
    new_state = (
        decay_rate[None, :, None, None] * prior_state
        + key_rot[:, :, :, None] * values[:, :, None, :]
    )
    state_read = jnp.einsum("bhk,bhkv->bhv", query_rot, new_state, precision=lax.Precision.HIGHEST)
    normed = state_read * lax.rsqrt(
        jnp.mean(state_read * state_read, axis=-1, keepdims=True) + norm_eps
    )
    gated_out = (
        (normed * jax.nn.silu(gate_pre))
        .astype(jnp.bfloat16)
        .reshape(own_rows, heads_here * VAL_DIM)
    )
    head_terms = rounded_product(lax.all_gather(gated_out, "ep", axis=0, tiled=True), out_weight)
    attn_out = lax.psum(head_terms.astype(jnp.float32).astype(jnp.bfloat16), "tp").astype(
        jnp.float32
    )
    after_mixer = (residual_float + attn_out).astype(jnp.bfloat16)
    capacity = max(2, 2 * own_rows * topk_count // ep_count)
    slot_count = ep_count * capacity
    target = slot_index(route_ids, ep_count, capacity, ep_count)
    slot_source = source_rows(target, batch_rows, topk_count, ep_count * slot_count)
    padded = jnp.concatenate([after_mixer, jnp.zeros((1, local_width), jnp.bfloat16)], axis=0)
    outgoing = padded[slot_source].reshape(ep_count, slot_count, local_width)
    arrived = lax.all_to_all(outgoing, "ep", split_axis=0, concat_axis=2, tiled=True)[0]
    rows_float = arrived.astype(jnp.float32)
    row_norm = lax.rsqrt(jnp.mean(rows_float * rows_float, axis=1, keepdims=True) + norm_eps)
    normed_rows = (rows_float * ffn_gain).astype(jnp.bfloat16)
    gate_val = jnp.minimum(
        jnp.dot(normed_rows, expert_gate[0], preferred_element_type=jnp.float32) * row_norm,
        clamp_limit,
    )
    up_val = jnp.clip(
        jnp.dot(normed_rows, expert_up[0], preferred_element_type=jnp.float32) * row_norm,
        -clamp_limit,
        clamp_limit,
    )
    hidden = ((up_val + 1.0) * gate_val * jax.nn.sigmoid(gate_alpha * gate_val)).astype(
        jnp.bfloat16
    )
    expert_part = rounded_product(hidden, expert_down[0]).astype(jnp.float32)
    expert_sum = lax.psum(expert_part.astype(jnp.bfloat16), "tp")
    returned = lax.all_to_all(expert_sum[None], "ep", split_axis=2, concat_axis=0, tiled=True)
    picked = returned.reshape(ep_count * slot_count, local_width)[target]
    picked = picked.reshape(batch_rows, topk_count, local_width).astype(jnp.float32)
    routed = jnp.sum(picked * route_weight[:, :, None], axis=1)
    after_float = after_mixer.astype(jnp.float32)
    gain_here = lax.dynamic_slice_in_dim(ffn_gain, ep_index * local_width, local_width, 0)
    normed_ffn = (after_float * gain_here).astype(jnp.bfloat16)
    dense_cols = dense_gate.shape[1]
    both_terms = jnp.dot(
        normed_ffn,
        jnp.concatenate([dense_gate, dense_up], axis=1),
        preferred_element_type=jnp.float32,
    )
    mix_term = jnp.dot(normed_ffn, mix_vector, preferred_element_type=jnp.float32)
    both_terms, ffn_squares, mix_logit = lax.psum(
        (both_terms, jnp.sum(after_float * after_float, axis=1), mix_term), "ep"
    )
    ffn_scale = lax.rsqrt(ffn_squares / D + norm_eps)[:, None]
    dense_act = (
        jax.nn.silu(both_terms[:, :dense_cols] * ffn_scale)
        * (both_terms[:, dense_cols:] * ffn_scale)
    ).astype(jnp.bfloat16)
    dense_part = rounded_product(dense_act, dense_down).astype(jnp.float32)
    dense_out = lax.psum(dense_part.astype(jnp.bfloat16), "tp").astype(jnp.float32)
    dense_mix = jax.nn.sigmoid(ffn_scale[:, 0] * mix_logit)
    layer_out = (after_float + routed + dense_mix[:, None] * dense_out).astype(jnp.bfloat16)
    return (layer_out, new_state)


def solution(mesh):
    placed = (
        P(None, "ep"),
        P("ep"),
        P("ep", "tp"),
        P("ep", "tp"),
        P("ep", "tp"),
        P("ep", "tp"),
        P("tp", "ep"),
        P("ep", "tp", None, None),
        P("ep"),
        P(),
        P("ep", None, "tp"),
        P("ep", None, "tp"),
        P("ep", "tp", None),
        P(),
        P(),
        P("ep", "tp"),
        P("ep", "tp"),
        P("tp", "ep"),
        P("ep"),
    )
    return jax.shard_map(
        per_device,
        mesh=mesh,
        in_specs=placed,
        out_specs=(P(None, "ep"), P("ep", "tp", None, None)),
        check_vma=False,
    )
```

profile of v0, /device:TPU:0, one launch (start us, length us, event | category | flops | bytes accessed | tf_op | source)
XLA Modules:
  0.0 276.0 jit_solution(3012465422165266415)
XLA Ops:
  7.2 0.0 reduce-scatter.2.cloned.1.call-start
  7.3 2.8 %fusion.5 = f32[64,3072]{1,0:T(8,128)} fusion(bf16[256,1024]{1,0:T(8,128)(2,1)} %param.26, bf16[256,1024]{1,0:T(8,128)(2,1)} %param.25, bf16[256,512]{1,0:T(8,128)(2,1)} %param.24, bf16[256,512]{1,0:T(8,128)(2,1)} %param.23, bf16[64,256]{1,0:T(8,128)(2,1)} %param.21, f32[256]{0:T(256)} %param.22), kind=kOutput, calls=%fused_computation.10 | convolution fusion | flops 107003904 | bytes 2393088 | tf_op jit(solution)/shard_map/dot_general | solution.py:83
  10.1 0.1 copy.46
  10.2 0.1 eq.15
  10.3 0.1 copy.47
  10.3 0.7 fusion.94
  11.1 0.1 copy.48
  11.2 0.1 reduce_sum.59
  11.3 0.1 copy.45
  11.4 0.1 mul.339
  11.5 0.1 add.155
  11.6 0.1 add.156
  11.6 0.6 dynamic-slice
  12.9 1.4 scatter_custom_fusion
  14.3 0.1 fusion.56
  14.4 23.3 %all-reduce.1 = f32[64]{0:T(128)S(1)} all-reduce(f32[64]{0:T(128)S(1)} %fusion.56), channel_id=3, replica_groups=mesh['ep'=8,'tp'=4] {'ep'}, use_global_device_ids=true, to_apply=%region_2.0.clone | all-reduce | flops 64 | bytes 512
  37.7 0.1 fusion.84
  37.8 0.1 fusion.82
  37.9 0.1 multiply_cosine_fusion
  38.0 39.9 %reduce-scatter.2.cloned.1.call-done = f32[8,3072]{1,0:T(8,128)} async-done(((f32[64,3072]{1,0:T(8,128)}), f32[8,3072]{1,0:T(8,128)}) %reduce-scatter.2.cloned.1.call-update) | async-done | bytes 98320 | tf_op jit(solution)/shard_map/reduce_scatter | solution.py:85
  77.9 1.0 broadcast_multiply_fusion
  78.9 0.1 multiply_subtract_fusion.1
  79.0 0.1 maximum_multiply_fusion
  79.1 0.1 maximum_bitcast_fusion
  79.1 2.6 multiply_add_fusion
  81.8 2.0 copy-done.1
  83.8 2.1 fusion.78
  85.9 0.1 fusion.72
  86.0 0.1 fusion.74
  86.1 30.6 %all_gather.3 = bf16[64,1024]{1,0:T(8,128)(2,1)S(1)} all-gather(bf16[8,1024]{1,0:T(8,128)(2,1)S(1)} %bitcast.91), channel_id=1, replica_groups=mesh['ep'=8,'tp'=4] {'ep'}, dimensions={0}, use_global_device_ids=true | all-gather | bytes 147456 | tf_op jit(solution)/shard_map/all_gather | solution.py:116
  116.6 0.2 convolution_convert_fusion.2
  116.8 10.3 %psum.42 = bf16[64,256]{1,0:T(8,128)(2,1)S(1)} all-reduce(bf16[64,256]{1,0:T(8,128)(2,1)S(1)} %convolution_convert_fusion.2), channel_id=1, replica_groups=mesh['ep'=8,'tp'=4] {'tp'}, use_global_device_ids=true, to_apply=%region_4.6 | all-reduce | flops 16384 | bytes 65536 | tf_op jit(solution)/shard_map/psum | solution.py:117
  127.1 0.1 fusion.60
  127.2 2.6 gather_fusion
  129.8 3.4 %all-to-all-start = ((bf16[8,64,256]{2,1,0:T(8,128)(2,1)}), bf16[8,64,256]{2,1,0:T(8,128)(2,1)S(1)}, u32[]{:S(2)}, u32[]{:S(2)}) async-start(bf16[8,64,256]{2,1,0:T(8,128)(2,1)} %bitcast.9), calls=%async_computation.1 | async-start | bytes 524288 | tf_op jit(solution)/shard_map/all_to_all | solution.py:127
  133.3 0.0 all-reduce.6.cloned.1.call-start
  133.3 0.1 copy.53
  133.4 0.1 dynamic_slice.3
  133.5 9.1 %all-to-all-done = bf16[8,64,256]{2,1,0:T(8,128)(2,1)S(1)} async-done(((bf16[8,64,256]{2,1,0:T(8,128)(2,1)}), bf16[8,64,256]{2,1,0:T(8,128)(2,1)S(1)}, u32[]{:S(2)}, u32[]{:S(2)}) %all-to-all-start) | async-done | bytes 262176 | tf_op jit(solution)/shard_map/all_to_all | solution.py:127
  142.6 0.2 fusion.41
  142.9 2.1 fusion.31
  145.0 3.3 %convolution_convert_fusion = bf16[64,2048]{1,0:T(8,128)(2,1)} fusion(bf16[1,512,2048]{2,1,0:T(8,128)(2,1)S(1)} %copy-done, f32[64,512]{1,0:T(8,128)S(1)} %fusion.31, bf16[64,2048]{1,0:T(8,128)(2,1)S(1)} %bitcast.84, bf16[1,2048,512]{2,1,0:T(8,128)(2,1)} %param.32, f32[64]{0:T(128)S(1)} %add_rsqrt_fusion.2), kind=kOutput, calls=%fused_computation.4 | convolution fusion | flops 268894208 | bytes 4849920 | tf_op jit(solution)/shard_map/dot_general | solution.py:49
  148.2 0.0 all-reduce.6.cloned.1.call-update
  148.3 0.0 all-reduce.8.cloned.1.call-start
  148.3 0.9 fusion.42
  149.3 0.0 all-reduce.8.cloned.1.call-update
  149.3 0.1 convolution_bitcast_fusion
  149.4 19.6 %all-reduce.2 = (f32[64]{0:T(128)S(1)}, f32[64]{0:T(128)S(1)}) all-reduce(f32[64]{0:T(128)S(1)} %get-tuple-element.5, f32[64]{0:T(128)S(1)} %convolution_bitcast_fusion), channel_id=1, replica_groups=mesh['ep'=8,'tp'=4] {'ep'}, use_global_device_ids=true, to_apply=%region_12.14 | all-reduce | flops 128 | bytes 1024 | tf_op jit(solution)/shard_map/psum | solution.py:159
  169.0 10.2 %all-reduce.6.cloned.1.call-done = bf16[1,64,2048]{2,1,0:T(8,128)(2,1)} async-done(((bf16[1,64,2048]{2,1,0:T(8,128)(2,1)}), bf16[1,64,2048]{2,1,0:T(8,128)(2,1)}) %all-reduce.6.cloned.1.call-update) | async-done | bytes 262160 | tf_op jit(solution)/shard_map/psum | solution.py:144
  179.2 2.2 copy.50
  181.4 0.5 broadcast.219
  182.0 12.3 %reduce.2 = bf16[2048,64]{1,0:T(8,128)(2,1)} reduce(bf16[2048,1,64]{2,1,0:T(2,128)(2,1)S(1)} %bitcast.82, bf16[]{:T(256)} %broadcast.219), dimensions={1}, to_apply=%bitcast.70.reduce_sub_computation | reduce | bytes 524290
  194.3 2.2 reshape.233
  196.4 5.5 %all-to-all-start.1 = ((bf16[8,2,8192]{2,1,0:T(2,128)(2,1)}), bf16[8,2,8192]{2,1,0:T(2,128)(2,1)S(1)}, u32[]{:S(2)}, u32[]{:S(2)}) async-start(bf16[8,2,8192]{2,1,0:T(2,128)(2,1)} %reshape.233), calls=%async_computation.2 | async-start | bytes 524288 | tf_op jit(solution)/shard_map/all_to_all | solution.py:145
  202.0 52.5 %all-reduce.8.cloned.1.call-done = f32[64,1024]{1,0:T(8,128)} async-done(((f32[64,1024]{1,0:T(8,128)}), f32[64,1024]{1,0:T(8,128)}) %all-reduce.8.cloned.1.call-update) | async-done | bytes 262160 | tf_op jit(solution)/shard_map/psum | solution.py:159
  254.4 1.2 convolution_convert_fusion.1
  255.6 10.3 %psum.47 = bf16[64,256]{1,0:T(8,128)(2,1)S(1)} all-reduce(bf16[64,256]{1,0:T(8,128)(2,1)S(1)} %convolution_convert_fusion.1), channel_id=1, replica_groups=mesh['ep'=8,'tp'=4] {'tp'}, use_global_device_ids=true, to_apply=%region_15.17 | all-reduce | flops 16384 | bytes 65536 | tf_op jit(solution)/shard_map/psum | solution.py:168
  265.9 0.6 reshape.234
  266.5 0.6 copy.51
  267.2 0.1 copy.57
  267.3 1.2 gather_fusion.1
  268.4 0.1 reshape.199
  268.5 0.2 multiply_reduce_fusion
  268.8 0.7 fusion.59
  (50 shorter events, 0.3 us)
Async XLA Ops:
  7.2 137.8 %copy-start = (bf16[1,512,2048]{2,1,0:T(8,128)(2,1)S(1)}, bf16[1,512,2048]{2,1,0:T(8,128)(2,1)}, u32[]{:S(2)}) copy-start(bf16[1,512,2048]{2,1,0:T(8,128)(2,1)} %param.33) | copy-start | bytes 6291460
  7.2 4.5 %copy-start.12 = (u32[32]{0:T(128)S(1)}, u32[32]{0:T(128)}, u32[]{:S(2)}) copy-start(u32[32]{0:T(128)} %constant.105) | copy-start | bytes 388
  7.2 7.1 %copy-start.3 = (bf16[64,256]{1,0:T(8,128)(2,1)S(1)}, bf16[64,256]{1,0:T(8,128)(2,1)}, u32[]{:S(2)}) copy-start(bf16[64,256]{1,0:T(8,128)(2,1)} %param.21) | copy-start | bytes 98308
  7.2 2.9 %copy-start.5 = (s32[64,4]{0,1:T(4,128)S(1)}, s32[64,4]{0,1:T(4,128)}, u32[]{:S(2)}) copy-start(s32[64,4]{0,1:T(4,128)} %param.34) | copy-start | bytes 3076
  7.2 3.9 %copy-start.10 = (s32[8]{0:T(128)S(1)}, s32[8]{0:T(128)}, u32[]{:S(2)}) copy-start(s32[8]{0:T(128)} %param.29) | copy-start | bytes 100
  7.2 70.6 %reduce-scatter.2.cloned.1.call-start = ((), (), s32[]{:S(2)}) async-start(), calls=%async_computation.3 | async-start | bytes 884736 | tf_op jit(solution)/shard_map/reduce_scatter | solution.py:85
  81.8 2.0 copy-start.1
  83.8 32.9 %copy-start.2 = (bf16[1024,256]{1,0:T(8,128)(2,1)S(1)}, bf16[1024,256]{1,0:T(8,128)(2,1)}, u32[]{:S(2)}) copy-start(bf16[1024,256]{1,0:T(8,128)(2,1)} %param.27) | copy-start | bytes 1572868
  83.8 49.5 %copy-start.4 = (f32[2048]{0:T(1024)S(1)}, f32[2048]{0:T(1024)}, u32[]{:S(2)}) copy-start(f32[2048]{0:T(1024)} %param.30) | copy-start | bytes 24580
  83.8 49.6 %copy-start.6 = (f32[64,4]{0,1:T(4,128)S(1)}, f32[64,4]{0,1:T(4,128)}, u32[]{:S(2)}) copy-start(f32[64,4]{0,1:T(4,128)} %param.35) | copy-start | bytes 3076
  83.8 49.7 %copy-start.11 = (bf16[256]{0:T(256)(128)(2,1)S(1)}, bf16[256]{0:T(256)(128)(2,1)}, u32[]{:S(2)}) copy-start(bf16[256]{0:T(256)(128)(2,1)} %param.39) | copy-start | bytes 1540
  129.8 12.8 %all-to-all-start = ((bf16[8,64,256]{2,1,0:T(8,128)(2,1)}), bf16[8,64,256]{2,1,0:T(8,128)(2,1)S(1)}, u32[]{:S(2)}, u32[]{:S(2)}) async-start(bf16[8,64,256]{2,1,0:T(8,128)(2,1)} %bitcast.9), calls=%async_computation.1 | async-start | bytes 524288 | tf_op jit(solution)/shard_map/all_to_all | solution.py:127
  133.3 46.0 %all-reduce.6.cloned.1.call-start = ((), (), s32[]{:S(2)}) async-start(), calls=%async_computation.4 | async-start | bytes 524288 | tf_op jit(solution)/shard_map/psum | solution.py:144
  144.9 3.4 %copy-start.7 = (bf16[256,512]{1,0:T(8,128)(2,1)S(1)}, bf16[256,512]{1,0:T(8,128)(2,1)}, u32[]{:S(2)}) copy-start(bf16[256,512]{1,0:T(8,128)(2,1)} %param.37) | copy-start | bytes 786436
  145.0 3.4 %copy-start.8 = (bf16[256,512]{1,0:T(8,128)(2,1)S(1)}, bf16[256,512]{1,0:T(8,128)(2,1)}, u32[]{:S(2)}) copy-start(bf16[256,512]{1,0:T(8,128)(2,1)} %param.36) | copy-start | bytes 786436
  148.2 106.2 %copy-start.9 = (bf16[512,256]{1,0:T(8,128)(2,1)S(1)}, bf16[512,256]{1,0:T(8,128)(2,1)}, u32[]{:S(2)}) copy-start(bf16[512,256]{1,0:T(8,128)(2,1)} %param.38) | copy-start | bytes 786436
  148.3 106.1 %all-reduce.8.cloned.1.call-start = ((), (), s32[]{:S(2)}) async-start(), calls=%async_computation.5 | async-start | bytes 524288 | tf_op jit(solution)/shard_map/psum | solution.py:159
  196.4 69.5 %all-to-all-start.1 = ((bf16[8,2,8192]{2,1,0:T(2,128)(2,1)}), bf16[8,2,8192]{2,1,0:T(2,128)(2,1)S(1)}, u32[]{:S(2)}, u32[]{:S(2)}) async-start(bf16[8,2,8192]{2,1,0:T(2,128)(2,1)} %reshape.233), calls=%async_computation.2 | async-start | bytes 524288 | tf_op jit(solution)/shard_map/all_to_all | solution.py:145
Sparse Core Ops, SparseCore 0:
  11.9 65.9 reduce-scatter.1
  148.4 30.7 all-reduce.5
  182.6 71.7 all-reduce.7
where the time goes:
time: 277 us; the launch traced here: 276 us
  waiting for transfers between devices  112 us (40%)
  blocking collectives  93.9 us (34%)
  other arithmetic  18.7 us (7%)
  local copies, waits for them, and re-layouts  15.1 us (5%)
  between operations  14.8 us (5%)
  matrix products  12.7 us (5%)
  starting transfers between devices  9.07 us (3%)
    psum x1, waiting for transfers between devices, per_device(): lax.psum((both_terms, jnp.sum(after_float * after_float, axis=1), mix_ter...  52.5 us
    reduce_scatter x1, waiting for transfers between devices, per_device(): lax.psum_scatter(whole_terms, 'ep', scatter_dimension=0, tiled=True)  39.9 us
    all_gather x1, blocking collectives, per_device(): lax.all_gather(gated_out, 'ep', axis=0, tiled=True)  30.6 us
    unnamed x1, blocking collectives  23.3 us
    psum x1, blocking collectives, per_device(): lax.psum((both_terms, jnp.sum(after_float * after_float, axis=1), mix_ter...  19.6 us
    unnamed x1, other arithmetic  12.3 us
    psum x1, blocking collectives, per_device(): lax.psum(head_terms.astype(jnp.float32).astype(jnp.bfloat16), 'tp')  10.3 us
    psum x1, blocking collectives, per_device(): lax.psum(dense_part.astype(jnp.bfloat16), 'tp').astype(jnp.float32)  10.3 us
  transfers between devices with their start and end apart: 5, of which 4 were waited for; matrix products, arithmetic and copies ran while one was open for 9% of the time, Pallas kernels for 0%

commit v1 on v0

--- a/solution.py
+++ b/solution.py
@@ -1,6 +1,8 @@
 import jax
 import jax.numpy as jnp
 from jax import lax
+from jax.experimental import pallas as pl
+from jax.experimental.pallas import tpu as pltpu
 from jax.sharding import PartitionSpec as P
 
 D = 2048
@@ -171,6 +173,335 @@
     return (layer_out, new_state)
 
 
+F32 = jnp.float32
+BF16 = jnp.bfloat16
+MESH = pl.DeviceIdType.MESH
+PROJ, SQUARE, MIX, HEAD, ROWS, DENSE_SUM, DENSE_ACT, BACK = range(8)
+ATTN, FINAL = range(2)
+
+
+def fused_kernel(
+    residual, norm_gain, cosine, sine, gains, route_ids, route_weight, mix_own,
+    query_hbm, key_hbm, value_hbm, gate_hbm, out_hbm, prior_hbm,
+    egate_hbm, eup_hbm, edown_hbm, dgate_hbm, dup_hbm, ddown_hbm,
+    layer_out, key_out, value_out,
+    query_w, key_w, value_w, gate_w, out_w, prior, prior_half,
+    egate, eup, edown, dgate, dup, ddown,
+    proj_send, proj_recv, sq_send, sq_recv, mix_all, heads_all, attn_all,
+    rows_all, square_rows, dense_send, dense_recv, act_all, back_send, back_recv, final_all,
+    load_sem, send_sem, recv_sem, tp_send, tp_recv,
+):
+    ep, batch, width = rows_all.shape
+    tp = attn_all.shape[0]
+    own = batch // ep
+    full = ep * width
+    me = lax.axis_index("ep")
+    lane = lax.axis_index("tp")
+    pairs = [
+        (query_hbm, query_w), (key_hbm, key_w), (value_hbm, value_w), (gate_hbm, gate_w),
+        (prior_hbm, prior), (out_hbm, out_w), (dgate_hbm, dgate), (dup_hbm, dup),
+        (egate_hbm, egate), (eup_hbm, eup), (edown_hbm, edown), (ddown_hbm, ddown),
+    ]
+    loads = [pltpu.make_async_copy(a, b, load_sem.at[i]) for i, (a, b) in enumerate(pairs)]
+    barrier = pltpu.get_barrier_semaphore()
+    for d in range(1, ep):
+        pl.semaphore_signal(
+            barrier, inc=1, device_id=(lax.rem(me + d, ep), lane), device_id_type=MESH
+        )
+    for d in range(1, tp):
+        pl.semaphore_signal(
+            barrier, inc=1, device_id=(me, lax.rem(lane + d, tp)), device_id_type=MESH
+        )
+    for load in loads:
+        load.start()
+
+    def to_ep(phase, d, source, target):
+        return pltpu.make_async_remote_copy(
+            src_ref=source,
+            dst_ref=target,
+            send_sem=send_sem.at[phase, d],
+            recv_sem=recv_sem.at[phase, d],
+            device_id=(lax.rem(me + d, ep), lane),
+            device_id_type=MESH,
+        )
+
+    def to_tp(phase, d, source, target):
+        return pltpu.make_async_remote_copy(
+            src_ref=source,
+            dst_ref=target,
+            send_sem=tp_send.at[phase, d],
+            recv_sem=tp_recv.at[phase, d],
+            device_id=(me, lax.rem(lane + d, tp)),
+            device_id_type=MESH,
+        )
+
+    sent = []
+
+    def go(copy):
+        copy.start()
+        sent.append(copy)
+
+    def peer(d):
+        return lax.rem(me + d, ep)
+
+    def sender(d):
+        return lax.rem(me + ep - d, ep)
+
+    def got(phase, d, buffer):
+        to_ep(phase, d, buffer, buffer).wait_recv()
+
+    resid = residual[...].astype(F32)
+    squares = jnp.sum(resid * resid, axis=1, keepdims=True)
+    squares = jnp.broadcast_to(squares, (batch, sq_send.shape[2]))
+    for e in range(ep):
+        sq_send[e] = squares[e * own : (e + 1) * own]
+    normed_in = (resid * norm_gain[...]).astype(BF16)
+    offset = 0
+    for load, weight in zip(loads[:4], (query_w, key_w, value_w, gate_w)):
+        load.wait()
+        cols = weight.shape[1]
+        step = min(cols, 512)
+        for c in range(0, cols, step):
+            terms = jnp.dot(normed_in, weight[:, c : c + step], preferred_element_type=F32)
+            for e in range(ep):
+                proj_send[e, :, offset + c : offset + c + step] = terms[
+                    e * own : (e + 1) * own
+                ].astype(BF16)
+        offset += cols
+    mix_all[me] = mix_own[...]
+    pl.semaphore_wait(barrier, ep + tp - 2)
+    for d in range(1, ep):
+        go(to_ep(SQUARE, d, sq_send.at[peer(d)], sq_recv.at[d]))
+        go(to_ep(PROJ, d, proj_send.at[peer(d)], proj_recv.at[d]))
+    for d in range(1, ep):
+        go(to_ep(MIX, d, mix_own, mix_all.at[me]))
+    heads = prior.shape[1]
+    loads[4].wait()
+    for b in range(own):
+        for h in range(heads):
+            prior_half[b, h] = prior[b, h].astype(BF16)
+    route_col = jnp.sum(
+        jnp.where(route_ids[...] == me, route_weight[...], 0.0), axis=1, keepdims=True
+    )
+    total_sq = sq_send[me]
+    projected = proj_send[me].astype(F32)
+    for d in range(1, ep):
+        got(SQUARE, d, sq_recv.at[d])
+        total_sq = total_sq + sq_recv[d]
+        got(PROJ, d, proj_recv.at[d])
+        projected = projected + proj_recv[d].astype(F32)
+    projected = projected * lax.rsqrt(total_sq / full + norm_eps)[:, :1]
+    key_cols = query_w.shape[1]
+    value_cols = value_w.shape[1]
+    value_out[...] = projected[:, 2 * key_cols : 2 * key_cols + value_cols]
+    row_ids = lax.broadcasted_iota(jnp.int32, (own, VAL_DIM), 0)
+    for h in range(heads):
+        ks = slice(h * KEY_DIM, (h + 1) * KEY_DIM)
+        q = projected[:, ks]
+        k = projected[:, key_cols + h * KEY_DIM : key_cols + (h + 1) * KEY_DIM]
+        q = q * cosine[...] + pltpu.roll(q, KEY_DIM // 2, 1) * sine[...]
+        k = (k * cosine[...] + pltpu.roll(k, KEY_DIM // 2, 1) * sine[...]) * KEY_DIM ** (-0.5)
+        key_out[:, ks] = k
+        start = 2 * key_cols + h * VAL_DIM
+        v = projected[:, start : start + VAL_DIM]
+        gate_pre = projected[:, start + value_cols : start + value_cols + VAL_DIM]
+        q_half = q.astype(BF16)
+        past = jnp.zeros((own, VAL_DIM), F32)
+        for b in range(own):
+            every = jnp.dot(q_half, prior_half[b, h], preferred_element_type=F32)
+            past = past + jnp.where(row_ids == b, every, 0.0)
+        head_id = jnp.full((own, VAL_DIM), lane * heads + h, jnp.int32).astype(F32)
+        decay = 1.0 - jnp.exp((head_id * 0.5 + 1.0) * -0.6931471805599453)
+        read = decay * past + jnp.sum(q * k, axis=1, keepdims=True) * v
+        normed = read * lax.rsqrt(jnp.mean(read * read, axis=1, keepdims=True) + norm_eps)
+        heads_all[me, :, h * VAL_DIM : (h + 1) * VAL_DIM] = (
+            normed * (gate_pre / (1.0 + jnp.exp(-gate_pre)))
+        ).astype(BF16)
+
+    for d in range(1, ep):
+        go(to_ep(HEAD, d, heads_all.at[me], heads_all.at[me]))
+    loads[5].wait()
+    for d in range(1, ep):
+        got(HEAD, d, heads_all.at[sender(d)])
+    gated = jnp.concatenate([heads_all[e].astype(F32) for e in range(ep)], axis=0)
+    attn_all[lane] = jnp.dot(
+        gated.astype(BF16), out_w[...], preferred_element_type=F32
+    ).astype(BF16)
+    for d in range(1, tp):
+        go(to_tp(ATTN, d, attn_all.at[lane], attn_all.at[lane]))
+    for d in range(1, tp):
+        slot = attn_all.at[lax.rem(lane + tp - d, tp)]
+        to_tp(ATTN, d, slot, slot).wait_recv()
+    attn = attn_all[0].astype(F32)
+    for t in range(1, tp):
+        attn = attn + attn_all[t].astype(F32)
+    after = (resid + attn).astype(BF16)
+    rows_all[me] = after
+    for d in range(1, ep):
+        go(to_ep(ROWS, d, rows_all.at[me], rows_all.at[me]))
+
+    after_float = after.astype(F32)
+    own_normed = (after_float * gains[me]).astype(BF16)
+    dense_cols = dgate.shape[1]
+    for i, weight in enumerate((dgate, dup)):
+        loads[6 + i].wait()
+        terms = jnp.dot(own_normed, weight[...], preferred_element_type=F32)
+        for e in range(ep):
+            dense_send[e, :, i * dense_cols : (i + 1) * dense_cols] = terms[
+                e * own : (e + 1) * own
+            ].astype(BF16)
+    for d in range(1, ep):
+        go(to_ep(DENSE_SUM, d, dense_send.at[peer(d)], dense_recv.at[d]))
+
+    loads[8].wait()
+    loads[9].wait()
+    gate_acc = up_acc = None
+    sq_acc = logit = None
+    for d in range(ep):
+        e = sender(d)
+        if d:
+            got(ROWS, d, rows_all.at[e])
+            got(MIX, d, mix_all.at[e])
+        z = rows_all[e].astype(F32)
+        zn = (z * gains[e]).astype(BF16)
+        depth = pl.ds(pl.multiple_of(e * width, width), width)
+        g = jnp.dot(zn, egate[0, depth, :], preferred_element_type=F32)
+        u = jnp.dot(zn, eup[0, depth, :], preferred_element_type=F32)
+        s = jnp.sum(z * z, axis=1, keepdims=True)
+        m = jnp.sum(zn.astype(F32) * mix_all[e], axis=1, keepdims=True)
+        if d:
+            gate_acc, up_acc, sq_acc, logit = gate_acc + g, up_acc + u, sq_acc + s, logit + m
+        else:
+            gate_acc, up_acc, sq_acc, logit = g, u, s, m
+    scale = lax.rsqrt(sq_acc / full + norm_eps)
+    square_rows[...] = jnp.broadcast_to(scale, square_rows.shape)
+    both = dense_send[me].astype(F32)
+    for d in range(1, ep):
+        got(DENSE_SUM, d, dense_recv.at[d])
+        both = both + dense_recv[d].astype(F32)
+    both = both * square_rows[pl.ds(pl.multiple_of(me * own, own), own), :][:, :1]
+    dg = both[:, :dense_cols]
+    act_all[me] = (dg / (1.0 + jnp.exp(-dg)) * both[:, dense_cols:]).astype(BF16)
+    for d in range(1, ep):
+        go(to_ep(DENSE_ACT, d, act_all.at[me], act_all.at[me]))
+    gate_val = jnp.minimum(gate_acc * scale, clamp_limit)
+    up_val = jnp.clip(up_acc * scale, -clamp_limit, clamp_limit)
+    hidden = ((up_val + 1.0) * gate_val / (1.0 + jnp.exp(-gate_alpha * gate_val))).astype(BF16)
+    loads[10].wait()
+    for d in list(range(1, ep)) + [0]:
+        e = peer(d)
+        columns = pl.ds(pl.multiple_of(e * width, width), width)
+        part = jnp.dot(hidden, edown[0, :, columns], preferred_element_type=F32) * route_col
+        if d:
+            back_send[d] = part.astype(BF16)
+            go(to_ep(BACK, d, back_send.at[d], back_recv.at[d]))
+    mixed = part
+    loads[11].wait()
+    for d in range(1, ep):
+        got(DENSE_ACT, d, act_all.at[sender(d)])
+    act = jnp.concatenate([act_all[e].astype(F32) for e in range(ep)], axis=0)
+    dense_part = jnp.dot(act.astype(BF16), ddown[...], preferred_element_type=F32)
+    mixed = mixed + dense_part / (1.0 + jnp.exp(-(scale * logit)))
+    for d in range(1, ep):
+        got(BACK, d, back_recv.at[d])
+        mixed = mixed + back_recv[d].astype(F32)
+    final_all[lane] = mixed.astype(BF16)
+    for d in range(1, tp):
+        go(to_tp(FINAL, d, final_all.at[lane], final_all.at[lane]))
+    for d in range(1, tp):
+        slot = final_all.at[lax.rem(lane + tp - d, tp)]
+        to_tp(FINAL, d, slot, slot).wait_recv()
+    result = after_float
+    for t in range(tp):
+        result = result + final_all[t].astype(F32)
+    layer_out[...] = result.astype(BF16)
+    for copy in sent:
+        copy.wait_send()
+
+
+def fused_device(
+    residual, norm_gain, query_weight, key_weight, value_weight, gate_weight, out_weight,
+    prior_state, lengths, ffn_gain, expert_gate, expert_up, expert_down, route_ids,
+    route_weight, dense_gate, dense_up, dense_down, mix_vector,
+):
+    ep, tp = lax.axis_size("ep"), lax.axis_size("tp")
+    batch, width = residual.shape
+    own, heads = prior_state.shape[:2]
+    half = KEY_DIM // 2
+    inverse = 1.0 / 10000.0 ** jnp.linspace(0.0, 1.0, half, dtype=F32)
+    angles = lengths.astype(F32)[:, None] * inverse[None, :]
+    cosine, sine = jnp.cos(angles), jnp.sin(angles)
+    cosine = jnp.concatenate([cosine, cosine], axis=1)
+    sine = jnp.concatenate([-sine, sine], axis=1)
+    key_cols, value_cols = query_weight.shape[1], value_weight.shape[1]
+    all_cols = 2 * key_cols + 2 * value_cols
+    dense_cols = dense_gate.shape[1]
+    large = (
+        query_weight, key_weight, value_weight, gate_weight, out_weight, prior_state,
+        expert_gate, expert_up, expert_down, dense_gate, dense_up, dense_down,
+    )
+    held = [pltpu.VMEM(a.shape, a.dtype) for a in large]
+    held.insert(6, pltpu.VMEM(prior_state.shape, BF16))
+    vmem = pl.BlockSpec(memory_space=pltpu.VMEM)
+    scratch = held + [
+        pltpu.VMEM((ep, own, all_cols), BF16),
+        pltpu.VMEM((ep, own, all_cols), BF16),
+        pltpu.VMEM((ep, own, 128), F32),
+        pltpu.VMEM((ep, own, 128), F32),
+        pltpu.VMEM((ep, 1, width), F32),
+        pltpu.VMEM((ep, own, value_cols), BF16),
+        pltpu.VMEM((tp, batch, width), BF16),
+        pltpu.VMEM((ep, batch, width), BF16),
+        pltpu.VMEM((batch, 128), F32),
+        pltpu.VMEM((ep, own, 2 * dense_cols), BF16),
+        pltpu.VMEM((ep, own, 2 * dense_cols), BF16),
+        pltpu.VMEM((ep, own, dense_cols), BF16),
+        pltpu.VMEM((ep, batch, width), BF16),
+        pltpu.VMEM((ep, batch, width), BF16),
+        pltpu.VMEM((tp, batch, width), BF16),
+        pltpu.SemaphoreType.DMA((12,)),
+        pltpu.SemaphoreType.DMA((8, ep)),
+        pltpu.SemaphoreType.DMA((8, ep)),
+        pltpu.SemaphoreType.DMA((2, tp)),
+        pltpu.SemaphoreType.DMA((2, tp)),
+    ]
+    layer_out, key_rot, values = pl.pallas_call(
+        fused_kernel,
+        out_shape=(
+            jax.ShapeDtypeStruct((batch, width), BF16),
+            jax.ShapeDtypeStruct((own, key_cols), F32),
+            jax.ShapeDtypeStruct((own, value_cols), F32),
+        ),
+        in_specs=[vmem] * 8 + [pl.BlockSpec(memory_space=pl.ANY)] * 12,
+        out_specs=(vmem, vmem, vmem),
+        scratch_shapes=scratch,
+        compiler_params=pltpu.CompilerParams(
+            collective_id=0, has_side_effects=True, vmem_limit_bytes=56 * 1024 * 1024
+        ),
+    )(
+        residual, norm_gain[None, :], cosine, sine, ffn_gain.reshape(ep, 1, width),
+        route_ids, route_weight, mix_vector.astype(F32)[None, :], *large,
+    )
+    head_ids = lax.axis_index("tp") * heads + jnp.arange(heads, dtype=jnp.int32)
+    decay_rate = 1.0 - jnp.exp2(-1.0 - 0.5 * head_ids.astype(F32))
+    key_rot = key_rot.reshape(own, heads, KEY_DIM)
+    values = values.reshape(own, heads, VAL_DIM)
+    new_state = (
+        decay_rate[None, :, None, None] * prior_state
+        + key_rot[:, :, :, None] * values[:, :, None, :]
+    )
+    return (layer_out, new_state)
+
+
+def any_device(*arrays):
+    residual, prior_state, dense_gate = arrays[0], arrays[7], arrays[15]
+    own = prior_state.shape[0]
+    aligned = residual.shape[1] % 128 == 0 and dense_gate.shape[1] % 128 == 0 and own % 8 == 0
+    if aligned:
+        return fused_device(*arrays)
+    return per_device(*arrays)
+
+
 def solution(mesh):
     placed = (
         P(None, "ep"),
@@ -194,7 +525,7 @@
         P("ep"),
     )
     return jax.shard_map(
-        per_device,
+        any_device,
         mesh=mesh,
         in_specs=placed,
         out_specs=(P(None, "ep"), P("ep", "tp", None, None)),

time: 277 us -> 61.4 us (0.22)
  waiting for transfers between devices: 112 us -> 0 us
  blocking collectives: 93.9 us -> 0 us
  Pallas kernels: 0 us -> 50.3 us
  between operations: 14.8 us -> 0.67 us
  other arithmetic: 18.7 us -> 5.18 us
  matrix products: 12.7 us -> 0 us
  local copies, waits for them, and re-layouts: 15.1 us -> 4.88 us
  starting transfers between devices: 9.07 us -> 0 us
    psum x2 -> x0, waiting for transfers between devices: 62.7 us -> none  [the longest x1 52.5 us: per_device(): lax.psum((both_terms, jnp.sum(after_float * after_float, axis=1), mix_ter...]
    pallas_call x0 -> x1, Pallas kernels: none -> 50.3 us  [fused_device(): pl.pallas_call(fused_kernel, out_shape=(jax.ShapeDtypeStruct((batch, widt...]
    psum x3 -> x0, blocking collectives: 40.1 us -> none  [the longest x1 19.6 us: per_device(): lax.psum((both_terms, jnp.sum(after_float * after_float, axis=1), mix_ter...]
    reduce_scatter x1 -> x0, waiting for transfers between devices: 39.9 us -> none  [per_device(): lax.psum_scatter(whole_terms, 'ep', scatter_dimension=0, tiled=True)]
    all_gather x1 -> x0, blocking collectives: 30.6 us -> none  [per_device(): lax.all_gather(gated_out, 'ep', axis=0, tiled=True)]
    unnamed x1 -> x0, blocking collectives: 23.3 us -> none
    dot_general x8 -> x0, matrix products: 12.7 us -> none  [the longest x3 4.67 us: rounded_product(): jnp.dot(left_rows, right_rows, preferred_element_type=jnp.float32)]
    unnamed x1 -> x0, other arithmetic: 12.3 us -> none
  transfers between devices with their start and end apart: 5 -> 0, of which waited for: 4 -> 0; matrix products, arithmetic and copies ran while one was open for 9% -> 0% of each run, Pallas kernels for 0% -> 0%
where the time goes in v1:
time: 61.4 us; the launch traced here: 61.1 us
  Pallas kernels  50.3 us (82%)
  other arithmetic  5.18 us (8%)
  local copies, waits for them, and re-layouts  4.88 us (8%)
  between operations  0.67 us (1%)
    pallas_call x1, Pallas kernels, fused_device(): pl.pallas_call(fused_kernel, out_shape=(jax.ShapeDtypeStruct((batch, widt...  50.3 us
    unnamed x7, local copies, waits for them, and re-layouts  3.39 us
    add x1, other arithmetic, fused_device(): decay_rate[None, :, None, None] * prior_state  2.4 us
    mul x2, local copies, waits for them, and re-layouts, fused_device(): key_rot[:, :, :, None] * values[:, :, None, :]  1.49 us
    broadcast_in_dim x1, other arithmetic, fused_device(): mix_vector.astype(F32)[None, :]  1.23 us

profile of v1, /device:TPU:0, one launch (start us, length us, event | category | flops | bytes accessed | tf_op | source)
XLA Modules:
  0.0 61.1 jit_solution(7138131382782803953)
XLA Ops:
  0.6 0.7 %convert_element_type.11 = f32[8]{0:T(128)S(1)} convert(s32[8]{0:T(128)} %param.27) | non-fusion elementwise | flops 8 | bytes 64 | tf_op jit(solution)/shard_map/convert_element_type | solution.py:432
  1.3 0.1 fusion.1
  1.4 1.2 %broadcast_in_dim.16 = f32[256]{0:T(256)} convert(bf16[256]{0:T(256)(128)(2,1)} %param.37) | non-fusion elementwise | flops 256 | bytes 1536 | tf_op jit(solution)/shard_map/broadcast_in_dim | solution.py:483
  2.6 0.1 fusion
  2.7 0.7 %pad_maximum_fusion = (f32[8,128]{1,0:T(8,128)}, f32[8,128]{1,0:T(8,128)}) fusion(f32[8,64]{1,0:T(8,128)S(1)} %get-tuple-element.10, f32[8,64]{1,0:T(8,128)S(1)} %get-tuple-element.9, f32[8,64]{1,0:T(8,128)S(1)} %get-tuple-element.8), kind=kLoop, calls=%fused_computation.3 | loop fusion | flops 2048 | bytes 14336 | tf_op jit(solution)/shard_map/concatenate | solution.py:434
  3.4 1.4 %copy.21.route_ids = s32[64,4]{1,0:T(8,128)} copy(s32[64,4]{0,1:T(4,128)} %param.32) | data formatting | bytes 2048 | tf_op args[13]
  4.8 1.4 %copy.22.route_weight = f32[64,4]{1,0:T(8,128)} copy(f32[64,4]{0,1:T(4,128)} %param.33) | data formatting | bytes 2048 | tf_op args[14]
  6.2 0.0 copy-start
  6.2 50.3 %shard_map.194 = (bf16[64,256]{1,0:T(8,128)(2,1)}, f32[8,512]{1,0:T(8,128)}, f32[8,1024]{1,0:T(8,128)}) custom-call(bf16[64,256]{1,0:T(8,128)(2,1)} %residual.1, f32[1,256]{1,0:T(1,128)} %bitcast.8, f32[8,128]{1,0:T(8,128)} %get-tuple-element.11.cosine, f32[8,128]{1,0:T(8,128)} %get-tuple-element.12.sine, f32[8,1,256]{2,1,0:T(1,128)} %bitcast.7, ...), custom_call_target="tpu_custom_call" | custom-call | tf_op jit(solution)/shard_map/pallas_call | solution.py:468
  56.5 0.7 %copy.23 = f32[8,4,128]{2,1,0:T(4,128)S(1)} copy(f32[8,4,128]{2,0,1:T(8,128)} %bitcast.6) | data formatting | bytes 32768 | tf_op jit(solution)/shard_map/mul | solution.py:491
  57.3 0.8 %copy.24 = f32[8,4,256]{2,1,0:T(4,128)S(1)} copy(f32[8,4,256]{2,0,1:T(8,128)} %bitcast.5) | data formatting | bytes 65536 | tf_op jit(solution)/shard_map/mul | solution.py:491
  58.0 0.0 copy-done
  58.1 0.0 copy-start.1
  58.1 2.4 %multiply_add_fusion = f32[8,4,128,256]{3,2,1,0:T(8,128)} fusion(f32[8,4,128,256]{3,2,1,0:T(8,128)S(1)} %copy-done, f32[8,4,256]{2,1,0:T(4,128)S(1)} %copy.24, f32[8,4,128]{2,1,0:T(4,128)S(1)} %copy.23, f32[4]{0:T(128)S(1)} %exponential_subtract_fusion), kind=kLoop, calls=%fused_computation | loop fusion | flops 3145728 | bytes 8437776 | tf_op jit(solution)/shard_map/add | solution.py:490
  60.5 0.0 copy-done.1
  60.5 0.6 %copy.26 = bf16[64,256]{1,0:T(8,128)(2,1)} copy(bf16[64,256]{1,0:T(8,128)(2,1)S(1)} %copy-done.1) | data formatting | bytes 65536
  (2 shorter events, 0.0 us)
Async XLA Ops:
  6.2 51.9 %copy-start = (f32[8,4,128,256]{3,2,1,0:T(8,128)S(1)}, f32[8,4,128,256]{3,2,1,0:T(8,128)}, u32[]{:S(2)}) copy-start(f32[8,4,128,256]{3,2,1,0:T(8,128)} %prior_hbm.1) | copy-start | bytes 12582916
  58.1 2.4 %copy-start.1 = (bf16[64,256]{1,0:T(8,128)(2,1)S(1)}, bf16[64,256]{1,0:T(8,128)(2,1)}, u32[]{:S(2)}) copy-start(bf16[64,256]{1,0:T(8,128)(2,1)} %get-tuple-element.15) | copy-start | bytes 98308

commit v2 on v1

--- a/solution.py
+++ b/solution.py
@@ -176,7 +176,7 @@
 F32 = jnp.float32
 BF16 = jnp.bfloat16
 MESH = pl.DeviceIdType.MESH
-PROJ, SQUARE, MIX, HEAD, ROWS, DENSE_SUM, DENSE_ACT, BACK = range(8)
+PROJ, SQUARE, MIX, HEAD, ROWS, DENSE_SUM, DENSE_ACT, BACK, QUERY = range(9)
 ATTN, FINAL = range(2)
 
 
@@ -187,16 +187,20 @@
     layer_out, key_out, value_out,
     query_w, key_w, value_w, gate_w, out_w, prior, prior_half,
     egate, eup, edown, dgate, dup, ddown,
-    proj_send, proj_recv, sq_send, sq_recv, mix_all, heads_all, attn_all,
+    query_send, query_recv, proj_send, proj_recv, sq_send, sq_recv, mix_all, heads_all, attn_all,
     rows_all, square_rows, dense_send, dense_recv, act_all, back_send, back_recv, final_all,
     load_sem, send_sem, recv_sem, tp_send, tp_recv,
+    relay_send, relay_recv,
 ):
-    ep, batch, width = rows_all.shape
+    _, ep, part_rows, width = rows_all.shape
+    batch = 2 * part_rows
     tp = attn_all.shape[0]
     own = batch // ep
     full = ep * width
     me = lax.axis_index("ep")
     lane = lax.axis_index("tp")
+    core = lax.rem(lane, 2)
+    twin = lane + 1 - 2 * core
     pairs = [
         (query_hbm, query_w), (key_hbm, key_w), (value_hbm, value_w), (gate_hbm, gate_w),
         (prior_hbm, prior), (out_hbm, out_w), (dgate_hbm, dgate), (dup_hbm, dup),
@@ -212,7 +216,7 @@
         pl.semaphore_signal(
             barrier, inc=1, device_id=(me, lax.rem(lane + d, tp)), device_id_type=MESH
         )
-    for load in loads:
+    for load in loads[:4]:
         load.start()
 
     def to_ep(phase, d, source, target):
@@ -256,60 +260,87 @@
     for e in range(ep):
         sq_send[e] = squares[e * own : (e + 1) * own]
     normed_in = (resid * norm_gain[...]).astype(BF16)
-    offset = 0
-    for load, weight in zip(loads[:4], (query_w, key_w, value_w, gate_w)):
-        load.wait()
+    def project(weight, target, offset):
         cols = weight.shape[1]
         step = min(cols, 512)
         for c in range(0, cols, step):
             terms = jnp.dot(normed_in, weight[:, c : c + step], preferred_element_type=F32)
             for e in range(ep):
-                proj_send[e, :, offset + c : offset + c + step] = terms[
+                target[e, :, offset + c : offset + c + step] = terms[
                     e * own : (e + 1) * own
                 ].astype(BF16)
-        offset += cols
-    mix_all[me] = mix_own[...]
+
+    key_cols = query_w.shape[1]
+    value_cols = value_w.shape[1]
+    loads[0].wait()
+    project(query_w, query_send, 0)
+    loads[1].wait()
+    project(key_w, proj_send, 0)
+    mix_rows = mix_own[...].astype(F32)
+    for i in range(width // 128):
+        mix_all[me, :, i * 128 : (i + 1) * 128] = mix_rows[i : i + 1]
     pl.semaphore_wait(barrier, ep + tp - 2)
     for d in range(1, ep):
         go(to_ep(SQUARE, d, sq_send.at[peer(d)], sq_recv.at[d]))
+        go(to_ep(QUERY, d, query_send.at[peer(d)], query_recv.at[d]))
+    loads[2].wait()
+    project(value_w, proj_send, key_cols)
+    loads[3].wait()
+    project(gate_w, proj_send, key_cols + value_cols)
+    for d in range(1, ep):
         go(to_ep(PROJ, d, proj_send.at[peer(d)], proj_recv.at[d]))
     for d in range(1, ep):
-        go(to_ep(MIX, d, mix_own, mix_all.at[me]))
+        go(to_ep(MIX, d, mix_all.at[me], mix_all.at[me]))
+    loads[4].start()
     heads = prior.shape[1]
     loads[4].wait()
     for b in range(own):
         for h in range(heads):
             prior_half[b, h] = prior[b, h].astype(BF16)
-    route_col = jnp.sum(
-        jnp.where(route_ids[...] == me, route_weight[...], 0.0), axis=1, keepdims=True
-    )
+    for load in loads[5:]:
+        load.start()
+    route_row = jnp.sum(
+        jnp.where(route_ids[...] == me, route_weight[...], 0.0), axis=0, keepdims=True
+    )
+    diagonal = lax.broadcasted_iota(jnp.int32, (batch, batch), 0) == lax.broadcasted_iota(
+        jnp.int32, (batch, batch), 1
+    )
+    route_col = jnp.sum(jnp.where(diagonal, route_row, 0.0), axis=1, keepdims=True)
     total_sq = sq_send[me]
-    projected = proj_send[me].astype(F32)
+    queries = query_send[me].astype(F32)
     for d in range(1, ep):
         got(SQUARE, d, sq_recv.at[d])
         total_sq = total_sq + sq_recv[d]
-        got(PROJ, d, proj_recv.at[d])
-        projected = projected + proj_recv[d].astype(F32)
-    projected = projected * lax.rsqrt(total_sq / full + norm_eps)[:, :1]
-    key_cols = query_w.shape[1]
-    value_cols = value_w.shape[1]
-    value_out[...] = projected[:, 2 * key_cols : 2 * key_cols + value_cols]
+        got(QUERY, d, query_recv.at[d])
+        queries = queries + query_recv[d].astype(F32)
+    row_scale = lax.rsqrt(total_sq / full + norm_eps)[:, :1]
+    queries = queries * row_scale
     row_ids = lax.broadcasted_iota(jnp.int32, (own, VAL_DIM), 0)
+    rotated, pasts = [], []
     for h in range(heads):
-        ks = slice(h * KEY_DIM, (h + 1) * KEY_DIM)
-        q = projected[:, ks]
-        k = projected[:, key_cols + h * KEY_DIM : key_cols + (h + 1) * KEY_DIM]
+        q = queries[:, h * KEY_DIM : (h + 1) * KEY_DIM]
         q = q * cosine[...] + pltpu.roll(q, KEY_DIM // 2, 1) * sine[...]
-        k = (k * cosine[...] + pltpu.roll(k, KEY_DIM // 2, 1) * sine[...]) * KEY_DIM ** (-0.5)
-        key_out[:, ks] = k
-        start = 2 * key_cols + h * VAL_DIM
-        v = projected[:, start : start + VAL_DIM]
-        gate_pre = projected[:, start + value_cols : start + value_cols + VAL_DIM]
         q_half = q.astype(BF16)
         past = jnp.zeros((own, VAL_DIM), F32)
         for b in range(own):
             every = jnp.dot(q_half, prior_half[b, h], preferred_element_type=F32)
             past = past + jnp.where(row_ids == b, every, 0.0)
+        rotated.append(q)
+        pasts.append(past)
+    projected = proj_send[me].astype(F32)
+    for d in range(1, ep):
+        got(PROJ, d, proj_recv.at[d])
+        projected = projected + proj_recv[d].astype(F32)
+    projected = projected * row_scale
+    for h in range(heads):
+        q, past = rotated[h], pasts[h]
+        k = projected[:, h * KEY_DIM : (h + 1) * KEY_DIM]
+        k = (k * cosine[...] + pltpu.roll(k, KEY_DIM // 2, 1) * sine[...]) * KEY_DIM ** (-0.5)
+        key_out[:, h, :] = k
+        start = key_cols + h * VAL_DIM
+        v = projected[:, start : start + VAL_DIM]
+        value_out[:, h, :] = v
+        gate_pre = projected[:, start + value_cols : start + value_cols + VAL_DIM]
         head_id = jnp.full((own, VAL_DIM), lane * heads + h, jnp.int32).astype(F32)
         decay = 1.0 - jnp.exp((head_id * 0.5 + 1.0) * -0.6931471805599453)
         read = decay * past + jnp.sum(q * k, axis=1, keepdims=True) * v
@@ -336,9 +367,10 @@
     for t in range(1, tp):
         attn = attn + attn_all[t].astype(F32)
     after = (resid + attn).astype(BF16)
-    rows_all[me] = after
-    for d in range(1, ep):
-        go(to_ep(ROWS, d, rows_all.at[me], rows_all.at[me]))
+    rows_all[0, me] = after[:part_rows]
+    rows_all[1, me] = after[part_rows:]
+    for d in range(1, ep):
+        go(to_ep(ROWS, d, rows_all.at[core, me], rows_all.at[core, me]))
 
     after_float = after.astype(F32)
     own_normed = (after_float * gains[me]).astype(BF16)
@@ -355,14 +387,30 @@
 
     loads[8].wait()
     loads[9].wait()
+    def relay(d, source):
+        return pltpu.make_async_remote_copy(
+            src_ref=source,
+            dst_ref=source,
+            send_sem=relay_send.at[d],
+            recv_sem=relay_recv.at[d],
+            device_id=(me, twin),
+            device_id_type=MESH,
+        )
+
+    def pass_on(d):
+        got(ROWS, d, rows_all.at[core, sender(d)])
+        go(relay(d, rows_all.at[core, sender(d)]))
+
     gate_acc = up_acc = None
     sq_acc = logit = None
     for d in range(ep):
         e = sender(d)
+        if d + 1 < ep:
+            pass_on(d + 1)
         if d:
-            got(ROWS, d, rows_all.at[e])
+            relay(d, rows_all.at[1 - core, e]).wait_recv()
             got(MIX, d, mix_all.at[e])
-        z = rows_all[e].astype(F32)
+        z = jnp.concatenate([rows_all[0, e].astype(F32), rows_all[1, e].astype(F32)], axis=0)
         zn = (z * gains[e]).astype(BF16)
         depth = pl.ds(pl.multiple_of(e * width, width), width)
         g = jnp.dot(zn, egate[0, depth, :], preferred_element_type=F32)
@@ -434,7 +482,7 @@
     cosine = jnp.concatenate([cosine, cosine], axis=1)
     sine = jnp.concatenate([-sine, sine], axis=1)
     key_cols, value_cols = query_weight.shape[1], value_weight.shape[1]
-    all_cols = 2 * key_cols + 2 * value_cols
+    all_cols = key_cols + 2 * value_cols
     dense_cols = dense_gate.shape[1]
     large = (
         query_weight, key_weight, value_weight, gate_weight, out_weight, prior_state,
@@ -444,6 +492,8 @@
     held.insert(6, pltpu.VMEM(prior_state.shape, BF16))
     vmem = pl.BlockSpec(memory_space=pltpu.VMEM)
     scratch = held + [
+        pltpu.VMEM((ep, own, key_cols), BF16),
+        pltpu.VMEM((ep, own, key_cols), BF16),
         pltpu.VMEM((ep, own, all_cols), BF16),
         pltpu.VMEM((ep, own, all_cols), BF16),
         pltpu.VMEM((ep, own, 128), F32),
@@ -451,7 +501,7 @@
         pltpu.VMEM((ep, 1, width), F32),
         pltpu.VMEM((ep, own, value_cols), BF16),
         pltpu.VMEM((tp, batch, width), BF16),
-        pltpu.VMEM((ep, batch, width), BF16),
+        pltpu.VMEM((2, ep, batch // 2, width), BF16),
         pltpu.VMEM((batch, 128), F32),
         pltpu.VMEM((ep, own, 2 * dense_cols), BF16),
         pltpu.VMEM((ep, own, 2 * dense_cols), BF16),
@@ -460,17 +510,19 @@
         pltpu.VMEM((ep, batch, width), BF16),
         pltpu.VMEM((tp, batch, width), BF16),
         pltpu.SemaphoreType.DMA((12,)),
-        pltpu.SemaphoreType.DMA((8, ep)),
-        pltpu.SemaphoreType.DMA((8, ep)),
+        pltpu.SemaphoreType.DMA((9, ep)),
+        pltpu.SemaphoreType.DMA((9, ep)),
         pltpu.SemaphoreType.DMA((2, tp)),
         pltpu.SemaphoreType.DMA((2, tp)),
+        pltpu.SemaphoreType.DMA((ep,)),
+        pltpu.SemaphoreType.DMA((ep,)),
     ]
     layer_out, key_rot, values = pl.pallas_call(
         fused_kernel,
         out_shape=(
             jax.ShapeDtypeStruct((batch, width), BF16),
-            jax.ShapeDtypeStruct((own, key_cols), F32),
-            jax.ShapeDtypeStruct((own, value_cols), F32),
+            jax.ShapeDtypeStruct((own, heads, KEY_DIM), F32),
+            jax.ShapeDtypeStruct((own, heads, VAL_DIM), F32),
         ),
         in_specs=[vmem] * 8 + [pl.BlockSpec(memory_space=pl.ANY)] * 12,
         out_specs=(vmem, vmem, vmem),
@@ -480,12 +532,10 @@
         ),
     )(
         residual, norm_gain[None, :], cosine, sine, ffn_gain.reshape(ep, 1, width),
-        route_ids, route_weight, mix_vector.astype(F32)[None, :], *large,
+        route_ids.T, route_weight.T, mix_vector.reshape(-1, 128), *large,
     )
     head_ids = lax.axis_index("tp") * heads + jnp.arange(heads, dtype=jnp.int32)
     decay_rate = 1.0 - jnp.exp2(-1.0 - 0.5 * head_ids.astype(F32))
-    key_rot = key_rot.reshape(own, heads, KEY_DIM)
-    values = values.reshape(own, heads, VAL_DIM)
     new_state = (
         decay_rate[None, :, None, None] * prior_state
         + key_rot[:, :, :, None] * values[:, :, None, :]
@@ -496,7 +546,8 @@
 def any_device(*arrays):
     residual, prior_state, dense_gate = arrays[0], arrays[7], arrays[15]
     own = prior_state.shape[0]
-    aligned = residual.shape[1] % 128 == 0 and dense_gate.shape[1] % 128 == 0 and own % 8 == 0
+    even = lax.axis_size("tp") % 2 == 0 and residual.shape[0] % 32 == 0
+    aligned = even and residual.shape[1] % 128 == 0 and dense_gate.shape[1] % 128 == 0 and own % 8 == 0
     if aligned:
         return fused_device(*arrays)
     return per_device(*arrays)

time: 61.4 us -> 53.6 us (0.87)
  local copies, waits for them, and re-layouts: 4.88 us -> 0.62 us
  Pallas kernels: 50.3 us -> 47.3 us
    pallas_call x1, Pallas kernels: 50.3 us -> 47.3 us  [fused_device(): pl.pallas_call(fused_kernel, out_shape=(jax.ShapeDtypeStruct((batch, widt...]
    unnamed x7 -> x5, local copies, waits for them, and re-layouts: 3.39 us -> 0.62 us
    mul x2 -> x0, local copies, waits for them, and re-layouts: 1.49 us -> none  [fused_device(): key_rot[:, :, :, None] * values[:, :, None, :]]
    broadcast_in_dim x1 -> x0, other arithmetic: 1.23 us -> none  [fused_device(): mix_vector.astype(F32)[None, :]]
    add x1, other arithmetic: 2.4 us -> 3.13 us  [fused_device(): decay_rate[None, :, None, None] * prior_state]
where the time goes in v2:
time: 53.6 us; the launch traced here: 53.3 us
  Pallas kernels  47.3 us (88%)
  other arithmetic  4.68 us (9%)
  between operations  0.67 us (1%)
  local copies, waits for them, and re-layouts  0.62 us (1%)
    pallas_call x1, Pallas kernels, fused_device(): pl.pallas_call(fused_kernel, out_shape=(jax.ShapeDtypeStruct((batch, widt...  47.3 us
    add x1, other arithmetic, fused_device(): decay_rate[None, :, None, None] * prior_state  3.13 us

profile of v2, /device:TPU:0, one launch (start us, length us, event | category | flops | bytes accessed | tf_op | source)
XLA Modules:
  0.0 53.3 jit_solution(11365244956992190264)
XLA Ops:
  0.6 0.7 %convert_element_type.10 = f32[8]{0:T(128)S(1)} convert(s32[8]{0:T(128)} %param.27) | non-fusion elementwise | flops 8 | bytes 64 | tf_op jit(solution)/shard_map/convert_element_type | solution.py:480
  1.3 0.1 fusion.1
  1.4 0.1 fusion
  1.5 0.7 %pad_maximum_fusion = (f32[8,128]{1,0:T(8,128)}, f32[8,128]{1,0:T(8,128)}) fusion(f32[8,64]{1,0:T(8,128)S(1)} %get-tuple-element.10, f32[8,64]{1,0:T(8,128)S(1)} %get-tuple-element.9, f32[8,64]{1,0:T(8,128)S(1)} %get-tuple-element.8), kind=kLoop, calls=%fused_computation.3 | loop fusion | flops 2048 | bytes 14336 | tf_op jit(solution)/shard_map/concatenate | solution.py:482
  2.2 0.0 copy-start
  2.2 47.3 %shard_map.194 = (bf16[64,256]{1,0:T(8,128)(2,1)}, f32[8,4,128]{2,1,0:T(4,128)}, f32[8,4,256]{2,1,0:T(4,128)}) custom-call(bf16[64,256]{1,0:T(8,128)(2,1)} %residual.1, f32[1,256]{1,0:T(1,128)} %bitcast.8, f32[8,128]{1,0:T(8,128)} %get-tuple-element.11.cosine, f32[8,128]{1,0:T(8,128)} %get-tuple-element.12.sine, f32[8,1,256]{2,1,0:T(1,128)} %bitcast.5, ...), custom_call_target="tpu_custom_call" | custom-call | tf_op jit(solution)/shard_map/pallas_call | solution.py:520
  49.5 0.0 copy-done
  49.5 0.0 copy-start.1
  49.5 3.1 %multiply_add_fusion = f32[8,4,128,256]{3,2,1,0:T(8,128)} fusion(f32[8,4,128,256]{3,2,1,0:T(8,128)S(1)} %copy-done, f32[8,4,256]{2,1,0:T(4,128)} %get-tuple-element.7, f32[8,4,128]{2,1,0:T(4,128)} %get-tuple-element.6, f32[4]{0:T(128)S(1)} %exponential_subtract_fusion), kind=kLoop, calls=%fused_computation | loop fusion | flops 3145728 | bytes 8437776 | tf_op jit(solution)/shard_map/add | solution.py:540
  52.7 0.0 copy-done.1
  52.7 0.6 %copy.22 = bf16[64,256]{1,0:T(8,128)(2,1)} copy(bf16[64,256]{1,0:T(8,128)(2,1)S(1)} %copy-done.1) | data formatting | bytes 65536
  (2 shorter events, 0.0 us)
Async XLA Ops:
  2.2 47.3 %copy-start = (f32[8,4,128,256]{3,2,1,0:T(8,128)S(1)}, f32[8,4,128,256]{3,2,1,0:T(8,128)}, u32[]{:S(2)}) copy-start(f32[8,4,128,256]{3,2,1,0:T(8,128)} %prior_hbm.1) | copy-start | bytes 12582916
  49.5 3.1 %copy-start.1 = (bf16[64,256]{1,0:T(8,128)(2,1)S(1)}, bf16[64,256]{1,0:T(8,128)(2,1)}, u32[]{:S(2)}) copy-start(bf16[64,256]{1,0:T(8,128)(2,1)} %get-tuple-element.15) | copy-start | bytes 98308

commit v3 on v2

--- a/solution.py
+++ b/solution.py
@@ -190,7 +190,7 @@
     query_send, query_recv, proj_send, proj_recv, sq_send, sq_recv, mix_all, heads_all, attn_all,
     rows_all, square_rows, dense_send, dense_recv, act_all, back_send, back_recv, final_all,
     load_sem, send_sem, recv_sem, tp_send, tp_recv,
-    relay_send, relay_recv,
+    relay_send, relay_recv, twin_out, twin_in, kept, halves, twin_send, twin_recv,
 ):
     _, ep, part_rows, width = rows_all.shape
     batch = 2 * part_rows
@@ -317,9 +317,11 @@
     queries = queries * row_scale
     row_ids = lax.broadcasted_iota(jnp.int32, (own, VAL_DIM), 0)
     rotated, pasts = [], []
+    turn_cos = jnp.concatenate([cosine[...], cosine[...]], axis=1)
+    turn_sin = jnp.concatenate([-sine[...], sine[...]], axis=1)
     for h in range(heads):
         q = queries[:, h * KEY_DIM : (h + 1) * KEY_DIM]
-        q = q * cosine[...] + pltpu.roll(q, KEY_DIM // 2, 1) * sine[...]
+        q = q * turn_cos + pltpu.roll(q, KEY_DIM // 2, 1) * turn_sin
         q_half = q.astype(BF16)
         past = jnp.zeros((own, VAL_DIM), F32)
         for b in range(own):
@@ -335,7 +337,7 @@
     for h in range(heads):
         q, past = rotated[h], pasts[h]
         k = projected[:, h * KEY_DIM : (h + 1) * KEY_DIM]
-        k = (k * cosine[...] + pltpu.roll(k, KEY_DIM // 2, 1) * sine[...]) * KEY_DIM ** (-0.5)
+        k = (k * turn_cos + pltpu.roll(k, KEY_DIM // 2, 1) * turn_sin) * KEY_DIM ** (-0.5)
         key_out[:, h, :] = k
         start = key_cols + h * VAL_DIM
         v = projected[:, start : start + VAL_DIM]
@@ -436,33 +438,70 @@
     up_val = jnp.clip(up_acc * scale, -clamp_limit, clamp_limit)
     hidden = ((up_val + 1.0) * gate_val / (1.0 + jnp.exp(-gate_alpha * gate_val))).astype(BF16)
     loads[10].wait()
-    for d in list(range(1, ep)) + [0]:
-        e = peer(d)
-        columns = pl.ds(pl.multiple_of(e * width, width), width)
+    first = jnp.full((part_rows, width), core, jnp.int32) == 0
+
+    def split(whole):
+        low, high = whole[:part_rows], whole[part_rows:]
+        return jnp.where(first, low, high), jnp.where(first, high, low)
+
+    def to_twin(i, source, target):
+        return pltpu.make_async_remote_copy(
+            src_ref=source,
+            dst_ref=target,
+            send_sem=twin_send.at[i],
+            recv_sem=twin_recv.at[i],
+            device_id=(me, twin),
+            device_id_type=MESH,
+        )
+
+    def hand_over(i, whole):
+        mine, other = split(whole)
+        kept[i] = mine
+        twin_out[i] = other.astype(BF16)
+        go(to_twin(i, twin_out.at[i], twin_in.at[i]))
+
+    def joined(i):
+        to_twin(i, twin_in.at[i], twin_in.at[i]).wait_recv()
+        return kept[i] + twin_in[i].astype(F32)
+
+    def give_back(d):
+        back_send[d] = joined(d).astype(BF16)
+        go(to_ep(BACK, d, back_send.at[d], back_recv.at[d]))
+
+    turns = list(range(1, ep)) + [0]
+    lag = min(3, ep - 1)
+    for i, d in enumerate(turns):
+        columns = pl.ds(pl.multiple_of(peer(d) * width, width), width)
         part = jnp.dot(hidden, edown[0, :, columns], preferred_element_type=F32) * route_col
-        if d:
-            back_send[d] = part.astype(BF16)
-            go(to_ep(BACK, d, back_send.at[d], back_recv.at[d]))
-    mixed = part
+        hand_over(d, part)
+        if i >= lag:
+            give_back(turns[i - lag])
+    for d in turns[ep - lag : ep - 1]:
+        give_back(d)
     loads[11].wait()
     for d in range(1, ep):
         got(DENSE_ACT, d, act_all.at[sender(d)])
     act = jnp.concatenate([act_all[e].astype(F32) for e in range(ep)], axis=0)
     dense_part = jnp.dot(act.astype(BF16), ddown[...], preferred_element_type=F32)
-    mixed = mixed + dense_part / (1.0 + jnp.exp(-(scale * logit)))
+    hand_over(ep, dense_part / (1.0 + jnp.exp(-(scale * logit))))
+    mixed = joined(0) + joined(ep)
     for d in range(1, ep):
         got(BACK, d, back_recv.at[d])
         mixed = mixed + back_recv[d].astype(F32)
     final_all[lane] = mixed.astype(BF16)
-    for d in range(1, tp):
+    for d in range(2, tp, 2):
         go(to_tp(FINAL, d, final_all.at[lane], final_all.at[lane]))
-    for d in range(1, tp):
+    for d in range(2, tp, 2):
         slot = final_all.at[lax.rem(lane + tp - d, tp)]
         to_tp(FINAL, d, slot, slot).wait_recv()
-    result = after_float
-    for t in range(tp):
-        result = result + final_all[t].astype(F32)
-    layer_out[...] = result.astype(BF16)
+    result, _ = split(after_float)
+    for t in range(tp // 2):
+        result = result + final_all[core + 2 * t].astype(F32)
+    halves[core] = result.astype(BF16)
+    go(to_twin(ep + 1, halves.at[core], halves.at[core]))
+    to_twin(ep + 1, halves.at[1 - core], halves.at[1 - core]).wait_recv()
+    layer_out[:part_rows] = halves[0]
+    layer_out[part_rows:] = halves[1]
     for copy in sent:
         copy.wait_send()
 
@@ -479,8 +518,6 @@
     inverse = 1.0 / 10000.0 ** jnp.linspace(0.0, 1.0, half, dtype=F32)
     angles = lengths.astype(F32)[:, None] * inverse[None, :]
     cosine, sine = jnp.cos(angles), jnp.sin(angles)
-    cosine = jnp.concatenate([cosine, cosine], axis=1)
-    sine = jnp.concatenate([-sine, sine], axis=1)
     key_cols, value_cols = query_weight.shape[1], value_weight.shape[1]
     all_cols = key_cols + 2 * value_cols
     dense_cols = dense_gate.shape[1]
@@ -506,9 +543,9 @@
         pltpu.VMEM((ep, own, 2 * dense_cols), BF16),
         pltpu.VMEM((ep, own, 2 * dense_cols), BF16),
         pltpu.VMEM((ep, own, dense_cols), BF16),
-        pltpu.VMEM((ep, batch, width), BF16),
-        pltpu.VMEM((ep, batch, width), BF16),
-        pltpu.VMEM((tp, batch, width), BF16),
+        pltpu.VMEM((ep, batch // 2, width), BF16),
+        pltpu.VMEM((ep, batch // 2, width), BF16),
+        pltpu.VMEM((tp, batch // 2, width), BF16),
         pltpu.SemaphoreType.DMA((12,)),
         pltpu.SemaphoreType.DMA((9, ep)),
         pltpu.SemaphoreType.DMA((9, ep)),
@@ -516,6 +553,12 @@
         pltpu.SemaphoreType.DMA((2, tp)),
         pltpu.SemaphoreType.DMA((ep,)),
         pltpu.SemaphoreType.DMA((ep,)),
+        pltpu.VMEM((ep + 1, batch // 2, width), BF16),
+        pltpu.VMEM((ep + 1, batch // 2, width), BF16),
+        pltpu.VMEM((ep + 1, batch // 2, width), F32),
+        pltpu.VMEM((2, batch // 2, width), BF16),
+        pltpu.SemaphoreType.DMA((ep + 2,)),
+        pltpu.SemaphoreType.DMA((ep + 2,)),
     ]
     layer_out, key_rot, values = pl.pallas_call(
         fused_kernel,

time: 53.6 us -> 53 us (0.989)
    sin x0 -> x1, other arithmetic: none -> 0.71 us  [fused_device(): cosine, sine = (jnp.cos(angles), jnp.sin(angles))]
    concatenate x1 -> x0, other arithmetic: 0.68 us -> none  [fused_device(): cosine = jnp.concatenate([cosine, cosine], axis=1)]
where the time goes in v3:
time: 53 us; the launch traced here: 52.8 us
  Pallas kernels  46.9 us (88%)
  other arithmetic  4.61 us (9%)
  between operations  0.66 us (1%)
  local copies, waits for them, and re-layouts  0.62 us (1%)
    pallas_call x1, Pallas kernels, fused_device(): pl.pallas_call(fused_kernel, out_shape=(jax.ShapeDtypeStruct((batch, widt...  46.9 us
    add x1, other arithmetic, fused_device(): decay_rate[None, :, None, None] * prior_state  3.13 us

profile of v3, /device:TPU:0, one launch (start us, length us, event | category | flops | bytes accessed | tf_op | source)
XLA Modules:
  0.0 52.8 jit_solution(7261507074542957706)
XLA Ops:
  0.6 0.7 %convert_element_type.10 = f32[8]{0:T(128)S(1)} convert(s32[8]{0:T(128)} %param.27) | non-fusion elementwise | flops 8 | bytes 64 | tf_op jit(solution)/shard_map/convert_element_type | solution.py:519
  1.3 0.1 fusion
  1.4 0.7 %multiply_sine_fusion = (f32[8,64]{1,0:T(8,128)}, f32[8,64]{1,0:T(8,128)}) fusion(f32[64]{0:T(128)S(1)} %fusion, f32[8]{0:T(128)S(1)} %convert_element_type.10), kind=kLoop, calls=%fused_computation.1 | loop fusion | flops 512 | bytes 4384 | tf_op jit(solution)/shard_map/sin | solution.py:520
  2.1 0.0 copy-start
  2.1 46.9 %shard_map.194 = (bf16[64,256]{1,0:T(8,128)(2,1)}, f32[8,4,128]{2,1,0:T(4,128)}, f32[8,4,256]{2,1,0:T(4,128)}) custom-call(bf16[64,256]{1,0:T(8,128)(2,1)} %residual.1, f32[1,256]{1,0:T(1,128)} %bitcast.8, f32[8,64]{1,0:T(8,128)} %get-tuple-element.9.cosine, f32[8,64]{1,0:T(8,128)} %get-tuple-element.8.sine, f32[8,1,256]{2,1,0:T(1,128)} %bitcast.5, ...), custom_call_target="tpu_custom_call" | custom-call | tf_op jit(solution)/shard_map/pallas_call | solution.py:563
  49.0 0.0 copy-done
  49.0 0.0 copy-start.1
  49.0 3.1 %multiply_add_fusion = f32[8,4,128,256]{3,2,1,0:T(8,128)} fusion(f32[8,4,128,256]{3,2,1,0:T(8,128)S(1)} %copy-done, f32[8,4,256]{2,1,0:T(4,128)} %get-tuple-element.7, f32[8,4,128]{2,1,0:T(4,128)} %get-tuple-element.6, f32[4]{0:T(128)S(1)} %exponential_subtract_fusion), kind=kLoop, calls=%fused_computation | loop fusion | flops 3145728 | bytes 8437776 | tf_op jit(solution)/shard_map/add | solution.py:583
  52.2 0.0 copy-done.1
  52.2 0.6 %copy.22 = bf16[64,256]{1,0:T(8,128)(2,1)} copy(bf16[64,256]{1,0:T(8,128)(2,1)S(1)} %copy-done.1) | data formatting | bytes 65536
  (2 shorter events, 0.0 us)
Async XLA Ops:
  2.1 46.9 %copy-start = (f32[8,4,128,256]{3,2,1,0:T(8,128)S(1)}, f32[8,4,128,256]{3,2,1,0:T(8,128)}, u32[]{:S(2)}) copy-start(f32[8,4,128,256]{3,2,1,0:T(8,128)} %prior_hbm.1) | copy-start | bytes 12582916
  49.0 3.1 %copy-start.1 = (bf16[64,256]{1,0:T(8,128)(2,1)S(1)}, bf16[64,256]{1,0:T(8,128)(2,1)}, u32[]{:S(2)}) copy-start(bf16[64,256]{1,0:T(8,128)(2,1)} %get-tuple-element.12) | copy-start | bytes 98308
